TPU v7x, 32 devices: a whole 2x2x4 slice. The times are simulated.
32 devices in a mesh: fs: 8 (over z, y), tp: 4 (over x, core).
Axes of the slice: x: 2, y: 2, z: 4, core: 2. Of those that a mesh axis runs over, the one named last changes fastest.
Arguments:
- inputs: bfloat16 [24576, 2048], P('fs'), may hold values from -6 to 6
- cot_query: bfloat16 [24576, 2048], P('fs', 'tp'), may hold values from -0.09375 to 0.09375
- cot_value: bfloat16 [24576, 4096], P('fs', 'tp'), may hold values from -0.09375 to 0.09375
- proj_query: bfloat16 [2048, 256], replicated, may hold values from -0.375 to 0.375
- proj_value: bfloat16 [2048, 256], replicated, may hold values from -0.375 to 0.375
- w_query: float32 [2048, 2048], P('fs', 'tp'), may hold values from -6 to 6
- w_value: float32 [2048, 4096], P('fs', 'tp'), may hold values from -6 to 6
- m_query: float32 [256, 2048], P('fs', 'tp'), may hold values from -30 to 30
- m_value: float32 [256, 4096], P('fs', 'tp'), may hold values from -30 to 30
- v_query: float32 [256, 2048], P('fs', 'tp'), may hold values from 0.05 to 2
- v_value: float32 [256, 4096], P('fs', 'tp'), may hold values from 0.05 to 2
Outputs:
- new_query: float32 [2048, 2048], P('fs', 'tp')
- new_value: float32 [2048, 4096], P('fs', 'tp')
- copy_query: bfloat16 [2048, 2048], P(None, 'tp')
- copy_value: bfloat16 [2048, 4096], P(None, 'tp')
- first_query: float32 [256, 2048], P('fs', 'tp')
- first_value: float32 [256, 4096], P('fs', 'tp')
- second_query: float32 [256, 2048], P('fs', 'tp')
- second_value: float32 [256, 4096], P('fs', 'tp')
- step_query: float32 [2048, 2048], P('fs', 'tp')
- step_value: float32 [2048, 4096], P('fs', 'tp')
All inputs are finite; a program needn't handle non-finite values.
Results may differ from a plain program's by a relative error of at most 0.015.
Values may be sent and summed in bfloat16 or wider, within the bound.
A program may use at most 128 MiB of HBM per device.

v0:
```python
import jax
import jax.numpy as jnp
from jax import lax
from jax.sharding import PartitionSpec as P

RANK = 256
QK_W = 2048
V_W = 4096


beta_first = 0.9
beta_second = 0.95
adam_eps = 1e-08
norm_eps = 1e-06
step_rate = 0.05
decay_rate = 0.2


def moment_update(low, first, second):
    first_new = beta_first * first + (1.0 - beta_first) * low
    second_new = beta_second * second + (1.0 - beta_second) * low * low
    update = first_new / (jnp.sqrt(second_new) + adam_eps)
    return (first_new, second_new, update)


def lead_product(left, right):
    return lax.dot_general(
        left, right, (((0,), (0,)), ((), ())), preferred_element_type=jnp.float32
    )


def split_pair(values):
    upper = values.astype(jnp.bfloat16)
    lower = (values - upper.astype(jnp.float32)).astype(jnp.bfloat16)
    return (upper, lower)


def front_exact(factor, values):
    upper, lower = split_pair(values)
    return jnp.dot(factor, upper, preferred_element_type=jnp.float32) + jnp.dot(
        factor, lower, preferred_element_type=jnp.float32
    )


def on_device(
    inputs,
    cot_query,
    cot_value,
    proj_query,
    proj_value,
    w_query,
    w_value,
    m_query,
    m_value,
    v_query,
    v_value,
):
    rows = w_query.shape[0]
    width_query = cot_query.shape[1]
    offset = lax.axis_index("fs") * rows
    local_query = lax.dynamic_slice_in_dim(proj_query, offset, rows, 0)
    local_value = lax.dynamic_slice_in_dim(proj_value, offset, rows, 0)
    factor_query = proj_query
    factor_value = proj_value
    mixed_query = jnp.dot(inputs, factor_query, preferred_element_type=jnp.float32)
    mixed_value = jnp.dot(inputs, factor_value, preferred_element_type=jnp.float32)
    upper_query, lower_query = split_pair(mixed_query)
    upper_value, lower_value = split_pair(mixed_value)
    low = lax.psum_scatter(
        jnp.concatenate(
            [
                lead_product(upper_query, cot_query) + lead_product(lower_query, cot_query),
                lead_product(upper_value, cot_value) + lead_product(lower_value, cot_value),
            ],
            axis=1,
        ),
        "fs",
        scatter_dimension=0,
        tiled=True,
    )
    first_query, second_query, update_query = moment_update(low[:, :width_query], m_query, v_query)
    first_value, second_value, update_value = moment_update(low[:, width_query:], m_value, v_value)
    total = lax.psum(
        jnp.sum(update_query * update_query) + jnp.sum(update_value * update_value), ("fs", "tp")
    )
    scale = lax.rsqrt(total / (RANK * (QK_W + V_W)) + norm_eps)
    factor_query = local_query
    factor_value = local_value
    back_query = front_exact(factor_query, lax.all_gather(update_query, "fs", axis=0, tiled=True))
    back_value = front_exact(factor_value, lax.all_gather(update_value, "fs", axis=0, tiled=True))
    step_query = scale * back_query + decay_rate * w_query
    step_value = scale * back_value + decay_rate * w_value
    new_query = w_query - step_rate * step_query
    new_value = w_value - step_rate * step_value
    copy_query, copy_value = (
        lax.all_gather(new_query.astype(jnp.bfloat16), "fs", axis=0, tiled=True),
        lax.all_gather(new_value.astype(jnp.bfloat16), "fs", axis=0, tiled=True),
    )
    return (
        new_query,
        new_value,
        copy_query,
        copy_value,
        first_query,
        first_value,
        second_query,
        second_value,
        step_query,
        step_value,
    )


def solution(mesh):
    return jax.shard_map(
        on_device,
        mesh=mesh,
        in_specs=(
            P("fs", None),
            P("fs", "tp"),
            P("fs", "tp"),
            P(),
            P(),
            P("fs", "tp"),
            P("fs", "tp"),
            P("fs", "tp"),
            P("fs", "tp"),
            P("fs", "tp"),
            P("fs", "tp"),
        ),
        out_specs=(
            P("fs", "tp"),
            P("fs", "tp"),
            P(None, "tp"),
            P(None, "tp"),
            P("fs", "tp"),
            P("fs", "tp"),
            P("fs", "tp"),
            P("fs", "tp"),
            P("fs", "tp"),
            P("fs", "tp"),
        ),
        check_vma=False,
    )
```

profile of v0, /device:TPU:4, one launch (start us, length us, event | category | flops | bytes accessed | tf_op | source)
XLA Modules:
  0.0 307.6 jit_solution(8068620610718707140)
XLA Ops:
  7.2 0.0 copy-start
  7.2 0.0 reduce-scatter.2.cloned.1.call-start
  7.2 0.0 slice-start
  7.3 0.0 slice-start.1
  7.3 7.0 %fusion.32 = f32[3072,256]{1,0:T(8,128)S(1)} fusion(bf16[3072,2048]{1,0:T(8,128)(2,1)} %param.11, bf16[2048,256]{1,0:T(8,128)(2,1)} %param.14), kind=kOutput, calls=%fused_computation.48 | convolution fusion | flops 3221225472 | bytes 16777216 | tf_op jit(solution)/shard_map/dot_general | solution.py:65
  14.2 0.0 copy-done
  14.2 0.0 slice-start.2
  14.2 1.1 fusion.10
  15.3 0.0 copy-start.4
  15.3 0.0 slice-start.3
  15.3 1.0 fusion.6
  16.4 0.0 slice-done
  16.4 0.0 slice-done.1
  16.4 0.4 slice-done.2
  16.9 0.2 copy-done.4
  17.0 0.0 slice-start.4
  17.0 3.6 %fusion.33 = f32[3072,256]{1,0:T(8,128)S(1)} fusion(bf16[3072,2048]{1,0:T(8,128)(2,1)S(1)} %bitcast.9, bf16[2048,256]{1,0:T(8,128)(2,1)S(1)} %copy-done.4), kind=kOutput, calls=%fused_computation.49 | convolution fusion | flops 3221225472 | bytes 16777216 | tf_op jit(solution)/shard_map/dot_general | solution.py:66
  20.6 0.0 slice-done.3
  20.6 0.0 slice-done.4
  20.6 1.8 fusion.1
  22.4 1.8 convolution_add_fusion.1
  24.3 0.0 copy-start.2
  24.3 0.0 copy-start.3
  24.3 0.0 copy-start.5
  24.3 0.0 copy-start.6
  24.3 1.3 pad_maximum_fusion
  25.6 0.0 reduce-scatter.2.cloned.1.call-update
  25.6 0.0 all-gather.4.cloned.1.call-start
  25.7 66.1 %reduce-scatter.2.cloned.1.call-done = f32[32,1536]{1,0:T(8,128)} async-done(((f32[256,1536]{1,0:T(8,128)}), f32[32,1536]{1,0:T(8,128)}) %reduce-scatter.2.cloned.1.call-update) | async-done | bytes 196624 | tf_op jit(solution)/shard_map/reduce_scatter | solution.py:69
  91.7 0.0 copy-done.2
  91.7 0.0 copy-done.3
  91.8 2.3 multiply_reduce_fusion
  94.0 0.0 all-gather.4.cloned.1.call-update
  94.1 0.0 all-gather.6.cloned.1.call-start
  94.1 0.0 copy-done.5
  94.1 0.0 copy-done.6
  94.1 2.1 multiply_reduce_fusion.1
  97.5 41.8 %psum.7 = f32[]{:T(128)} all-reduce(f32[]{:T(128)S(6)} %add.66), channel_id=1, replica_groups=mesh['fs'=8,'tp'=4] {'fs','tp'}, use_global_device_ids=true, to_apply=%region_3.0 | all-reduce | flops 1 | bytes 8 | tf_op jit(solution)/shard_map/psum | solution.py:83
  140.0 30.1 %all_gather.12 = f32[256,512]{1,0:T(8,128)S(1)} all-gather(f32[32,512]{1,0:T(8,128)S(1)} %get-tuple-element.19), channel_id=1, replica_groups=mesh['fs'=8,'tp'=4] {'fs'}, dimensions={0}, use_global_device_ids=true | all-gather | bytes 589824 | tf_op jit(solution)/shard_map/all_gather | solution.py:89
  170.1 1.1 fusion.17
  171.2 2.5 fusion.29
  173.6 0.0 all-gather.6.cloned.1.call-update
  173.7 0.0 all-gather.8.cloned.1.call-start
  173.7 0.0 all-gather.4.cloned.1.call-done
  173.7 1.6 fusion.13
  175.4 3.8 %fusion.28 = (bf16[256,1024]{1,0:T(8,128)(2,1)}, f32[256,1024]{1,0:T(8,128)}, f32[256,1024]{1,0:T(8,128)}) fusion(f32[256,1024]{1,0:T(8,128)} %param.17, f32[256,1024]{1,0:T(8,128)S(1)} %fusion.13, f32[256,1024]{1,0:T(8,128)} %all-gather.4.cloned.1.call-done, bf16[2048,256]{1,0:T(8,128)(2,1)} %param.15, s32[]{:T(128)S(6)} %select_n.4, f32[]{:T(128)S(6)} %rsqrt.3), kind=kOutput, calls=%fused_computation.46 | convolution fusion | flops 137101312 | bytes 5898248 | tf_op jit(solution)/shard_map/dot_general | solution.py:40
  179.2 0.0 all-gather.8.cloned.1.call-update
  179.2 42.7 %all-gather.6.cloned.1.call-done = bf16[2048,512]{1,0:T(8,128)(2,1)} async-done(((bf16[256,512]{1,0:T(8,128)(2,1)}), bf16[2048,512]{1,0:T(8,128)(2,1)}) %all-gather.6.cloned.1.call-update) | async-done | bytes 2097168 | tf_op jit(solution)/shard_map/all_gather | solution.py:96
  221.9 73.9 %all-gather.8.cloned.1.call-done = bf16[2048,1024]{1,0:T(8,128)(2,1)} async-done(((bf16[256,1024]{1,0:T(8,128)(2,1)}), bf16[2048,1024]{1,0:T(8,128)(2,1)}) %all-gather.8.cloned.1.call-update) | async-done | bytes 4194320 | tf_op jit(solution)/shard_map/all_gather | solution.py:97
  295.8 0.0 copy-start.1
  295.8 3.2 %copy.23 = bf16[2048,512]{1,0:T(8,128)(2,1)} copy(bf16[2048,512]{1,0:T(8,128)(2,1)} %all-gather.6.cloned.1.call-done) | data formatting | bytes 4194304
  299.0 0.0 copy-done.1
  299.0 2.0 copy.24
  (2 shorter events, 0.0 us)
Async XLA Ops:
  7.2 7.0 %copy-start = (bf16[3072,512]{1,0:T(8,128)(2,1)S(1)}, bf16[3072,512]{1,0:T(8,128)(2,1)}, u32[]{:S(2)}) copy-start(bf16[3072,512]{1,0:T(8,128)(2,1)} %param.12) | copy-start | bytes 9437188
  7.2 84.6 %reduce-scatter.2.cloned.1.call-start = ((), (), s32[]{:S(2)}) async-start(), calls=%async_computation.1 | async-start | bytes 1769472 | tf_op jit(solution)/shard_map/reduce_scatter | solution.py:69
  7.2 9.1 %slice-start = ((s8[12582912]{0:T(1024)(128)(4,1)}), s8[4194304]{0:T(1024)(128)(4,1)S(1)}, s32[]{:S(2)}) async-start(s8[12582912]{0:T(1024)(128)(4,1)} %bitcast.8), calls=%async_computation.5 | async-start | bytes 8388608
  7.3 9.1 %slice-start.1 = ((s8[12582912]{0:T(1024)(128)(4,1)}), s8[4194304]{0:T(1024)(128)(4,1)S(1)}, s32[]{:S(2)}) async-start(s8[12582912]{0:T(1024)(128)(4,1)} %bitcast.8), calls=%async_computation.6 | async-start | bytes 8388608
  14.2 2.6 slice-start.2
  15.3 1.7 copy-start.4
  15.3 5.3 %slice-start.3 = ((s8[6291456]{0:T(1024)(128)(4,1)}), s8[4194304]{0:T(1024)(128)(4,1)S(1)}, s32[]{:S(2)}) async-start(s8[6291456]{0:T(1024)(128)(4,1)} %bitcast.10), calls=%async_computation.8 | async-start | bytes 8388608
  17.0 3.6 %slice-start.4 = ((s8[6291456]{0:T(1024)(128)(4,1)}), s8[2097152]{0:T(1024)(128)(4,1)S(1)}, s32[]{:S(2)}) async-start(s8[6291456]{0:T(1024)(128)(4,1)} %bitcast.10), calls=%async_computation.9 | async-start | bytes 4194304
  24.3 67.5 %copy-start.2 = (f32[32,1024]{1,0:T(8,128)S(1)}, f32[32,1024]{1,0:T(8,128)}, u32[]{:S(2)}) copy-start(f32[32,1024]{1,0:T(8,128)} %param.21) | copy-start | bytes 393220
  24.3 67.5 %copy-start.3 = (f32[32,1024]{1,0:T(8,128)S(1)}, f32[32,1024]{1,0:T(8,128)}, u32[]{:S(2)}) copy-start(f32[32,1024]{1,0:T(8,128)} %param.19) | copy-start | bytes 393220
  24.3 69.8 %copy-start.5 = (f32[32,512]{1,0:T(8,128)S(1)}, f32[32,512]{1,0:T(8,128)}, u32[]{:S(2)}) copy-start(f32[32,512]{1,0:T(8,128)} %param.20) | copy-start | bytes 196612
  24.3 69.8 %copy-start.6 = (f32[32,512]{1,0:T(8,128)S(1)}, f32[32,512]{1,0:T(8,128)}, u32[]{:S(2)}) copy-start(f32[32,512]{1,0:T(8,128)} %param.18) | copy-start | bytes 196612
  25.6 148.1 %all-gather.4.cloned.1.call-start = ((), (), s32[]{:S(2)}) async-start(), calls=%async_computation.2 | async-start | bytes 1179648 | tf_op jit(solution)/shard_map/all_gather | solution.py:90
  94.1 127.9 %all-gather.6.cloned.1.call-start = ((), (), s32[]{:S(2)}) async-start(), calls=%async_computation.3 | async-start | bytes 2359296 | tf_op jit(solution)/shard_map/all_gather | solution.py:96
  173.7 122.2 %all-gather.8.cloned.1.call-start = ((), (), s32[]{:S(2)}) async-start(), calls=%async_computation.4 | async-start | bytes 4718592 | tf_op jit(solution)/shard_map/all_gather | solution.py:97
  295.8 3.2 %copy-start.1 = (bf16[2048,1024]{1,0:T(8,128)(2,1)S(1)}, bf16[2048,1024]{1,0:T(8,128)(2,1)}, u32[]{:S(2)}) copy-start(bf16[2048,1024]{1,0:T(8,128)(2,1)} %all-gather.8.cloned.1.call-done) | copy-start | bytes 12582916
Sparse Core Ops, SparseCore 0:
  25.7 65.9 reduce-scatter.1
  94.4 39.1 all-gather.3
  173.8 48.0 all-gather.5
  224.5 71.3 all-gather.7
where the time goes:
time: 310 us; the launch traced here: 308 us
  waiting for transfers between devices  183 us (59%)
  blocking collectives  71.8 us (23%)
  matrix products  25.3 us (8%)
  between operations  16 us (5%)
  local copies, waits for them, and re-layouts  5.89 us (2%)
  other arithmetic  5.67 us (2%)
    all_gather x1, waiting for transfers between devices, on_device(): lax.all_gather(new_value.astype(jnp.bfloat16), 'fs', axis=0, tiled=True)  73.9 us
    reduce_scatter x1, waiting for transfers between devices, on_device(): lax.psum_scatter(jnp.concatenate([lead_product(upper_query, cot_query) +...  66.1 us
    all_gather x1, waiting for transfers between devices, on_device(): lax.all_gather(new_query.astype(jnp.bfloat16), 'fs', axis=0, tiled=True)  42.7 us
    psum x1, blocking collectives, on_device(): lax.psum(jnp.sum(update_query * update_query) + jnp.sum(update_value * up...  41.8 us
    all_gather x1, blocking collectives, on_device(): lax.all_gather(update_query, 'fs', axis=0, tiled=True)  30.1 us
    dot_general x1, matrix products, on_device(): jnp.dot(inputs, factor_query, preferred_element_type=jnp.float32)  6.95 us
    dot_general x2, matrix products, front_exact(): jnp.dot(factor, lower, preferred_element_type=jnp.float32)  6.28 us
  transfers between devices with their start and end apart: 4, of which 3 were waited for; matrix products, arithmetic and copies ran while one was open for 4% of the time, Pallas kernels for 0%

commit v1 on v0

v1 whole, which is shorter than its diff:
```python
import functools

import jax
import jax.numpy as jnp
from jax import lax
from jax.experimental import pallas as pl
from jax.experimental.pallas import tpu as pltpu
from jax.sharding import PartitionSpec as P

beta_first = 0.9
beta_second = 0.95
adam_eps = 1e-08
norm_eps = 1e-06
step_rate = 0.05
decay_rate = 0.2


def moments(low, first, second):
    first_new = beta_first * first + (1.0 - beta_first) * low
    second_new = beta_second * second + (1.0 - beta_second) * low * low
    return first_new, second_new


def update_of(low, first, second):
    first_new, second_new = moments(low, first, second)
    return first_new / (jnp.sqrt(second_new) + adam_eps)


def ring_order(n):
    if n % 4 or n < 8:
        return list(range(n))
    cols = n // 4
    cycle = [0]
    for z in range(4):
        span = range(1, cols) if z % 2 == 0 else range(cols - 1, 0, -1)
        cycle += [z * cols + y for y in span]
    return cycle + [z * cols for z in (3, 2, 1)]


def lookup(table, index):
    value = jnp.int32(table[0])
    for k in range(1, len(table)):
        value = jnp.where(index == k, jnp.int32(table[k]), value)
    return value


def kernel(
    n,
    t,
    tile,
    x_hbm,
    cq_hbm,
    cv_hbm,
    pq_ref,
    pv_ref,
    wq_ref,
    wv_ref,
    mq_ref,
    mv_ref,
    vq_ref,
    vv_ref,
    gq_hbm,
    gv_hbm,
    uq_ref,
    uv_ref,
    lowq_ref,
    lowv_ref,
    total_ref,
    acc_q,
    acc_v,
    part_q,
    part_v,
    got_q,
    got_v,
    sums,
    w_send,
    w_recv,
    own_sem,
    r_send,
    r_recv,
    u_send,
    u_recv,
    t_send,
    t_recv,
):
    me = lax.axis_index("fs")
    col = lax.axis_index("tp")
    order = ring_order(n)
    place = [order.index(k) for k in range(n)]
    pos = lookup(place, me)

    def at(step):
        return lookup(order, lax.rem(pos + step + 2 * n, n))

    rows = wq_ref.shape[0]
    half_rows = rows // 2
    ranks = mq_ref.shape[0]

    barrier = pltpu.get_barrier_semaphore()
    for d in range(1, n):
        pl.semaphore_signal(
            barrier, inc=1, device_id={"fs": lax.rem(me + d, n)}, device_id_type=pl.DeviceIdType.MESH
        )
    for d in range(1, t):
        pl.semaphore_signal(
            barrier, inc=1, device_id={"tp": lax.rem(col + d, t)}, device_id_type=pl.DeviceIdType.MESH
        )
    pl.semaphore_wait(barrier, n - 1 + t - 1)

    def reach(way, half):
        return n // 2 if way == half else n - 1 - n // 2

    sign = (1, -1)

    def w_copy(way, half, hop):
        owner = at(-sign[way] * hop)
        target = at(sign[way])
        copies = []
        for k, (own, out) in enumerate(((wq_ref, gq_hbm), (wv_ref, gv_hbm))):
            place_ = pl.ds(pl.multiple_of(owner * rows + half * half_rows, half_rows), half_rows)
            src = own.at[pl.ds(half * half_rows, half_rows)] if hop == 0 else out.at[place_]
            copies.append(
                pltpu.make_async_remote_copy(
                    src_ref=src,
                    dst_ref=out.at[place_],
                    send_sem=w_send.at[way, half, hop, k],
                    recv_sem=w_recv.at[way, half, hop, k],
                    device_id={"fs": target},
                    device_id_type=pl.DeviceIdType.MESH,
                )
            )
        return copies

    def w_arrived(way, half, hop):
        owner = at(-sign[way] * (hop + 1))
        for k, out in enumerate((gq_hbm, gv_hbm)):
            place_ = pl.ds(pl.multiple_of(owner * rows + half * half_rows, half_rows), half_rows)
            pltpu.make_async_remote_copy(
                src_ref=out.at[place_],
                dst_ref=out.at[place_],
                send_sem=w_send.at[way, half, hop, k],
                recv_sem=w_recv.at[way, half, hop, k],
                device_id={"fs": at(sign[way])},
                device_id_type=pl.DeviceIdType.MESH,
            ).wait_recv()

    started = []

    def send_w(hop):
        for half in range(2):
            for way in range(2):
                if hop and hop - 1 < reach(way, half):
                    w_arrived(way, half, hop - 1)
                if hop < reach(way, half):
                    for copy in w_copy(way, half, hop):
                        copy.start()
                        started.append(copy)

    send_w(0)
    mine = pl.ds(pl.multiple_of(me * rows, rows), rows)
    own = [
        pltpu.make_async_copy(wq_ref, gq_hbm.at[mine], own_sem.at[0]),
        pltpu.make_async_copy(wv_ref, gv_hbm.at[mine], own_sem.at[1]),
    ]
    for copy in own:
        copy.start()

    acc_q[...] = jnp.zeros_like(acc_q)
    acc_v[...] = jnp.zeros_like(acc_v)

    def lead(left, right):
        return lax.dot_general(
            left, right, (((0,), (0,)), ((), ())), preferred_element_type=jnp.float32
        )

    def body(x, cq, cv):
        values = x[...]
        mixed_q = jnp.dot(values, pq_ref[...], preferred_element_type=jnp.float32)
        acc_q[...] += lead(mixed_q.astype(jnp.bfloat16), cq[...])
        mixed_v = jnp.dot(values, pv_ref[...], preferred_element_type=jnp.float32)
        acc_v[...] += lead(mixed_v.astype(jnp.bfloat16), cv[...])

    pltpu.emit_pipeline(
        body,
        grid=(x_hbm.shape[0] // tile,),
        in_specs=[
            pl.BlockSpec((tile, x_hbm.shape[1]), lambda i: (i, 0)),
            pl.BlockSpec((tile, cq_hbm.shape[1]), lambda i: (i, 0)),
            pl.BlockSpec((tile, cv_hbm.shape[1]), lambda i: (i, 0)),
        ],
        out_specs=[],
    )(x_hbm, cq_hbm, cv_hbm)

    part_q[...] = acc_q[...].astype(jnp.bfloat16)
    part_v[...] = acc_v[...].astype(jnp.bfloat16)
    scattered = []
    for d in range(1, n):
        target = lax.rem(me + d, n)
        chunk = pl.ds(pl.multiple_of(target * ranks, ranks), ranks)
        for k, (part, got) in enumerate(((part_q, got_q), (part_v, got_v))):
            copy = pltpu.make_async_remote_copy(
                src_ref=part.at[chunk],
                dst_ref=got.at[d - 1],
                send_sem=r_send.at[d - 1, k],
                recv_sem=r_recv.at[d - 1, k],
                device_id={"fs": target},
                device_id_type=pl.DeviceIdType.MESH,
            )
            copy.start()
            scattered.append(copy)

    send_w(1)

    for copy in scattered:
        copy.wait_recv()
    kept = pl.ds(pl.multiple_of(me * ranks, ranks), ranks)
    for acc, got, low_ref, m_ref, v_ref, u_ref in (
        (acc_q, got_q, lowq_ref, mq_ref, vq_ref, uq_ref),
        (acc_v, got_v, lowv_ref, mv_ref, vv_ref, uv_ref),
    ):
        low = acc[kept, :]
        for d in range(n - 1):
            low = low + got[d].astype(jnp.float32)
        low_ref[...] = low
        u_ref[kept, :] = update_of(low, m_ref[...], v_ref[...]).astype(jnp.bfloat16)

    gathered = []
    for d in range(1, n):
        for k, u_ref in enumerate((uq_ref, uv_ref)):
            copy = pltpu.make_async_remote_copy(
                src_ref=u_ref.at[kept],
                dst_ref=u_ref.at[kept],
                send_sem=u_send.at[d - 1, k],
                recv_sem=u_recv.at[d - 1, k],
                device_id={"fs": lax.rem(me + d, n)},
                device_id_type=pl.DeviceIdType.MESH,
            )
            copy.start()
            gathered.append(copy)

    send_w(2)

    for d in range(1, n):
        source = lax.rem(me - d + n, n)
        chunk = pl.ds(pl.multiple_of(source * ranks, ranks), ranks)
        for k, u_ref in enumerate((uq_ref, uv_ref)):
            pltpu.make_async_remote_copy(
                src_ref=u_ref.at[chunk],
                dst_ref=u_ref.at[chunk],
                send_sem=u_send.at[d - 1, k],
                recv_sem=u_recv.at[d - 1, k],
                device_id={"fs": source},
                device_id_type=pl.DeviceIdType.MESH,
            ).wait_recv()

    square = jnp.float32(0)
    for u_ref in (uq_ref, uv_ref):
        values = u_ref[...].astype(jnp.float32)
        square = square + jnp.sum(values * values)
    sums[0] = jnp.full(sums.shape[1:], square, jnp.float32)
    shared = []
    for d in range(1, t):
        copy = pltpu.make_async_remote_copy(
            src_ref=sums.at[0],
            dst_ref=sums.at[d],
            send_sem=t_send.at[d - 1],
            recv_sem=t_recv.at[d - 1],
            device_id={"tp": lax.rem(col + d, t)},
            device_id_type=pl.DeviceIdType.MESH,
        )
        copy.start()
        shared.append(copy)

    for hop in range(3, n // 2 + 1):
        send_w(hop)

    for copy in shared:
        copy.wait_recv()
    total_ref[...] = jnp.sum(sums[...], axis=0)
    for copy in own:
        copy.wait()
    for copy in started + scattered + gathered + shared:
        copy.wait_send()


def on_device(n, t, inputs, cot_query, cot_value, proj_query, proj_value,
              w_query, w_value, m_query, m_value, v_query, v_value):
    depth = proj_query.shape[0]
    rank = proj_query.shape[1]
    ranks = m_query.shape[0]
    rows = w_query.shape[0]
    width_q = w_query.shape[1]
    width_v = w_value.shape[1]
    tokens = inputs.shape[0]
    tile = 512 if tokens % 512 == 0 else tokens
    half = jnp.bfloat16
    full = jnp.float32
    anywhere = pl.BlockSpec(memory_space=pl.ANY)
    inside = pl.BlockSpec(memory_space=pltpu.VMEM)
    hops = n // 2
    gq, gv, uq, uv, lowq, lowv, total = pl.pallas_call(
        functools.partial(kernel, n, t, tile),
        out_shape=(
            jax.ShapeDtypeStruct((depth, width_q), half),
            jax.ShapeDtypeStruct((depth, width_v), half),
            jax.ShapeDtypeStruct((rank, width_q), half),
            jax.ShapeDtypeStruct((rank, width_v), half),
            jax.ShapeDtypeStruct((ranks, width_q), full),
            jax.ShapeDtypeStruct((ranks, width_v), full),
            jax.ShapeDtypeStruct((8, 128), full),
        ),
        in_specs=[anywhere] * 3 + [inside] * 8,
        out_specs=(anywhere,) * 2 + (inside,) * 5,
        scratch_shapes=[
            pltpu.VMEM((rank, width_q), full),
            pltpu.VMEM((rank, width_v), full),
            pltpu.VMEM((rank, width_q), half),
            pltpu.VMEM((rank, width_v), half),
            pltpu.VMEM((n - 1, ranks, width_q), half),
            pltpu.VMEM((n - 1, ranks, width_v), half),
            pltpu.VMEM((t, 8, 128), full),
            pltpu.SemaphoreType.DMA((2, 2, hops, 2)),
            pltpu.SemaphoreType.DMA((2, 2, hops, 2)),
            pltpu.SemaphoreType.DMA((2,)),
            pltpu.SemaphoreType.DMA((n - 1, 2)),
            pltpu.SemaphoreType.DMA((n - 1, 2)),
            pltpu.SemaphoreType.DMA((n - 1, 2)),
            pltpu.SemaphoreType.DMA((n - 1, 2)),
            pltpu.SemaphoreType.DMA((t - 1,)),
            pltpu.SemaphoreType.DMA((t - 1,)),
        ],
        compiler_params=pltpu.CompilerParams(
            collective_id=0, has_side_effects=True, vmem_limit_bytes=48 * 2**20
        ),
    )(
        inputs, cot_query, cot_value, proj_query, proj_value,
        w_query.astype(half), w_value.astype(half),
        m_query, m_value, v_query, v_value,
    )
    first_query, second_query = moments(lowq, m_query, v_query)
    first_value, second_value = moments(lowv, m_value, v_value)
    count = rank * t * (width_q + width_v)
    scale = lax.rsqrt(total[0, 0] / count + norm_eps)
    offset = lax.axis_index("fs") * rows
    local_q = lax.dynamic_slice_in_dim(proj_query, offset, rows, 0)
    local_v = lax.dynamic_slice_in_dim(proj_value, offset, rows, 0)

    def dot(a, b):
        return jnp.dot(a, b, preferred_element_type=full)

    def whole(kept, factor, update):
        step = scale * dot(factor, update) + decay_rate * kept.astype(full)
        return (kept.astype(full) - step_rate * step).astype(half)

    step_query = scale * dot(local_q, uq) + decay_rate * w_query
    step_value = scale * dot(local_v, uv) + decay_rate * w_value
    new_query = w_query - step_rate * step_query
    new_value = w_value - step_rate * step_value
    return (
        new_query,
        new_value,
        whole(gq, proj_query, uq),
        whole(gv, proj_value, uv),
        first_query,
        first_value,
        second_query,
        second_value,
        step_query,
        step_value,
    )


def solution(mesh):
    n = mesh.shape["fs"]
    t = mesh.shape["tp"]
    split = P("fs", "tp")
    return jax.shard_map(
        functools.partial(on_device, n, t),
        mesh=mesh,
        in_specs=(P("fs", None), split, split, P(), P()) + (split,) * 6,
        out_specs=(split, split, P(None, "tp"), P(None, "tp")) + (split,) * 6,
        check_vma=False,
    )
```

time: 310 us -> 129 us (0.42)
  waiting for transfers between devices: 183 us -> 0 us
  Pallas kernels: 0 us -> 105 us
  blocking collectives: 71.8 us -> 0 us
  between operations: 16 us -> 1.39 us
  matrix products: 25.3 us -> 11.6 us
    all_gather x3 -> x0, waiting for transfers between devices: 117 us -> none  [the longest x1 73.9 us: on_device(): lax.all_gather(new_value.astype(jnp.bfloat16), 'fs', axis=0, tiled=True)]
    pallas_call x0 -> x1, Pallas kernels: none -> 105 us  [on_device(): pl.pallas_call(functools.partial(kernel, n, t, tile), out_shape=(jax.Shap...]
    reduce_scatter x1 -> x0, waiting for transfers between devices: 66.1 us -> none  [on_device(): lax.psum_scatter(jnp.concatenate([lead_product(upper_query, cot_query) +...]
    psum x1 -> x0, blocking collectives: 41.8 us -> none  [on_device(): lax.psum(jnp.sum(update_query * update_query) + jnp.sum(update_value * up...]
    all_gather x1 -> x0, blocking collectives: 30.1 us -> none  [on_device(): lax.all_gather(update_query, 'fs', axis=0, tiled=True)]
    dot_general x10 -> x4, matrix products: 25.3 us -> 11.6 us  [dot(): return jnp.dot(a, b, preferred_element_type=full)]
    reduce_sum x2 -> x0, other arithmetic: 4.4 us -> none  [the longest x1 2.28 us: on_device(): jnp.sum(update_value * update_value)]
  transfers between devices with their start and end apart: 4 -> 0, of which waited for: 3 -> 0; matrix products, arithmetic and copies ran while one was open for 4% -> 0% of each run, Pallas kernels for 0% -> 0%
where the time goes in v1:
time: 129 us; the launch traced here: 128 us
  Pallas kernels  105 us (81%)
  matrix products  11.6 us (9%)
  local copies, waits for them, and re-layouts  6.45 us (5%)
  other arithmetic  3.78 us (3%)
  between operations  1.39 us (1%)
    pallas_call x1, Pallas kernels, on_device(): pl.pallas_call(functools.partial(kernel, n, t, tile), out_shape=(jax.Shap...  105 us
    dot_general x4, matrix products, dot(): return jnp.dot(a, b, preferred_element_type=full)  11.6 us
    unnamed x18, local copies, waits for them, and re-layouts  5.94 us

profile of v1, /device:TPU:4, one launch (start us, length us, event | category | flops | bytes accessed | tf_op | source)
XLA Modules:
  0.0 128.4 jit_solution(14192828506229083450)
XLA Ops:
  0.6 1.1 convert_element_type.20.wq_ref
  1.7 1.3 %convert_element_type.21.wv_ref = bf16[256,1024]{1,0:T(8,128)(2,1)S(1)} convert(f32[256,1024]{1,0:T(8,128)} %param.17) | non-fusion elementwise | flops 262144 | bytes 1572864 | tf_op jit(solution)/shard_map/convert_element_type | solution.py:337
  3.0 0.0 copy-start
  3.0 1.2 copy-done
  4.3 0.0 copy-start.1
  4.3 1.2 copy-done.1
  5.5 0.0 copy-start.2
  5.5 0.9 copy-done.2
  6.4 0.0 copy-start.3
  6.4 0.9 copy-done.3
  7.3 0.0 copy-start.4
  7.3 0.8 copy-done.4
  8.1 0.0 copy-start.5
  8.1 0.8 copy-done.5
  9.0 105.3 %shard_map.186 = (bf16[2048,512]{1,0:T(8,128)(2,1)}, bf16[2048,1024]{1,0:T(8,128)(2,1)}, bf16[256,512]{1,0:T(8,128)(2,1)S(1)}, bf16[256,1024]{1,0:T(8,128)(2,1)S...) custom-call(bf16[3072,2048]{1,0:T(8,128)(2,1)} %x_hbm.1, bf16[3072,512]{1,0:T(8,128)(2,1)} %cq_hbm.1, ...), custom_call_target="tpu_custom_call" | custom-call | tf_op jit(solution)/shard_map/pallas_call | solution.py:301
  114.2 0.5 slice.3
  115.5 0.0 copy-start.8
  115.5 6.3 %fusion.2 = bf16[2048,1024]{1,0:T(8,128)(2,1)} fusion(bf16[2048,1024]{1,0:T(8,128)(2,1)} %get-tuple-element.21, bf16[2048,256]{1,0:T(8,128)(2,1)S(1)} %copy-done.1, bf16[256,1024]{1,0:T(8,128)(2,1)S(1)} %get-tuple-element.19, f32[]{:T(128)} %bitcast), kind=kOutput, calls=%fused_computation.4 | convolution fusion | flops 1088421888 | bytes 9961476 | tf_op jit(solution)/shard_map/dot_general | solution.py:349
  121.8 0.0 copy-done.8
  121.8 0.0 copy-start.7
  121.8 0.0 copy-start.6
  121.8 2.3 %fusion.5 = bf16[2048,512]{1,0:T(8,128)(2,1)} fusion(bf16[2048,512]{1,0:T(8,128)(2,1)S(1)} %copy-done.8, bf16[2048,256]{1,0:T(8,128)(2,1)S(1)} %copy-done, bf16[256,512]{1,0:T(8,128)(2,1)S(1)} %get-tuple-element.18, f32[]{:T(128)} %bitcast), kind=kOutput, calls=%fused_computation.9 | convolution fusion | flops 544210944 | bytes 5505028 | tf_op jit(solution)/shard_map/dot_general | solution.py:349
  124.1 0.7 fusion.11
  124.8 0.7 fusion.8
  125.5 0.0 copy-done.7
  125.5 1.2 multiply_subtract_fusion.1
  126.8 0.0 copy-done.6
  126.8 1.7 %multiply_subtract_fusion = (f32[256,1024]{1,0:T(8,128)}, f32[256,1024]{1,0:T(8,128)}) fusion(f32[256,1024]{1,0:T(8,128)S(1)} %copy-done.6, bf16[256,1024]{1,0:T(8,128)(2,1)S(1)} %get-tuple-element.19, bf16[2048,256]{1,0:T(8,128)(2,1)S(1)} %copy-done.1, s32[]{:T(128)S(6)} %select_n.4, f32[]{:T(128)} %bitcast), kind=kOutput, calls=%fused_computation.14 | convolution fusion | flops 135528448 | bytes 3801096 | tf_op jit(solution)/shard_map/dot_general | solution.py:349
Async XLA Ops:
  3.0 1.2 copy-start
  4.3 1.2 copy-start.1
  5.5 0.9 copy-start.2
  6.4 0.9 copy-start.3
  7.3 0.8 copy-start.4
  8.1 0.8 copy-start.5
  115.5 6.3 %copy-start.8 = (bf16[2048,512]{1,0:T(8,128)(2,1)S(1)}, bf16[2048,512]{1,0:T(8,128)(2,1)}, u32[]{:S(2)}) copy-start(bf16[2048,512]{1,0:T(8,128)(2,1)} %get-tuple-element.20) | copy-start | bytes 6291460
  121.8 3.8 %copy-start.7 = (f32[256,512]{1,0:T(8,128)S(1)}, f32[256,512]{1,0:T(8,128)}, u32[]{:S(2)}) copy-start(f32[256,512]{1,0:T(8,128)} %param.16) | copy-start | bytes 1572868
  121.8 5.0 %copy-start.6 = (f32[256,1024]{1,0:T(8,128)S(1)}, f32[256,1024]{1,0:T(8,128)}, u32[]{:S(2)}) copy-start(f32[256,1024]{1,0:T(8,128)} %param.17) | copy-start | bytes 3145732

commit v2 on v1

--- a/solution.py
+++ b/solution.py
@@ -51,14 +51,14 @@
     x_hbm,
     cq_hbm,
     cv_hbm,
-    pq_ref,
-    pv_ref,
+    pq_hbm,
+    pv_hbm,
     wq_ref,
     wv_ref,
-    mq_ref,
-    mv_ref,
-    vq_ref,
-    vv_ref,
+    mq_hbm,
+    mv_hbm,
+    vq_hbm,
+    vv_hbm,
     gq_hbm,
     gv_hbm,
     uq_ref,
@@ -70,9 +70,22 @@
     acc_v,
     part_q,
     part_v,
+    near_q,
+    near_v,
     got_q,
     got_v,
     sums,
+    pq_ref,
+    pv_ref,
+    mq_ref,
+    mv_ref,
+    vq_ref,
+    vv_ref,
+    load_sem,
+    y_send,
+    y_recv,
+    f_send,
+    f_recv,
     w_send,
     w_recv,
     own_sem,
@@ -146,8 +159,8 @@
 
     started = []
 
-    def send_w(hop):
-        for half in range(2):
+    def send_w(hop, halves=(0, 1)):
+        for half in halves:
             for way in range(2):
                 if hop and hop - 1 < reach(way, half):
                     w_arrived(way, half, hop - 1)
@@ -162,11 +175,27 @@
         pltpu.make_async_copy(wq_ref, gq_hbm.at[mine], own_sem.at[0]),
         pltpu.make_async_copy(wv_ref, gv_hbm.at[mine], own_sem.at[1]),
     ]
-    for copy in own:
+    loads = [
+        pltpu.make_async_copy(src, dst, load_sem.at[k])
+        for k, (src, dst) in enumerate(
+            (
+                (pq_hbm, pq_ref),
+                (pv_hbm, pv_ref),
+                (mq_hbm, mq_ref),
+                (mv_hbm, mv_ref),
+                (vq_hbm, vq_ref),
+                (vv_hbm, vv_ref),
+            )
+        )
+    ]
+    for copy in loads + own:
         copy.start()
 
     acc_q[...] = jnp.zeros_like(acc_q)
     acc_v[...] = jnp.zeros_like(acc_v)
+
+    for copy in loads:
+        copy.wait()
 
     def lead(left, right):
         return lax.dot_general(
@@ -191,27 +220,68 @@
         out_specs=[],
     )(x_hbm, cq_hbm, cv_hbm)
 
-    part_q[...] = acc_q[...].astype(jnp.bfloat16)
-    part_v[...] = acc_v[...].astype(jnp.bfloat16)
-    scattered = []
-    for d in range(1, n):
-        target = lax.rem(me + d, n)
-        chunk = pl.ds(pl.multiple_of(target * ranks, ranks), ranks)
-        for k, (part, got) in enumerate(((part_q, got_q), (part_v, got_v))):
-            copy = pltpu.make_async_remote_copy(
-                src_ref=part.at[chunk],
-                dst_ref=got.at[d - 1],
-                send_sem=r_send.at[d - 1, k],
-                recv_sem=r_recv.at[d - 1, k],
-                device_id={"fs": target},
-                device_id_type=pl.DeviceIdType.MESH,
+    zs, ys = part_q.shape[:2]
+    my_z, my_y = me // ys, lax.rem(me, ys)
+    pairs = ((acc_q, part_q, near_q, got_q), (acc_v, part_v, near_v, got_v))
+
+    def remote(src, dst, send, recv, target):
+        return pltpu.make_async_remote_copy(
+            src_ref=src,
+            dst_ref=dst,
+            send_sem=send,
+            recv_sem=recv,
+            device_id={"fs": target},
+            device_id_type=pl.DeviceIdType.MESH,
+        )
+
+    for acc, part, near, got in pairs:
+        for z in range(zs):
+            for y in range(ys):
+                start = (z * ys + y) * ranks
+                part[z, y] = acc[start : start + ranks, :].astype(jnp.bfloat16)
+    across = []
+    for d in range(1, ys):
+        other = lax.rem(my_y + d, ys)
+        for k, (acc, part, near, got) in enumerate(pairs):
+            copy = remote(
+                part.at[:, other],
+                near.at[d - 1],
+                y_send.at[d - 1, k],
+                y_recv.at[d - 1, k],
+                my_z * ys + other,
             )
             copy.start()
-            scattered.append(copy)
-
-    send_w(1)
-
-    for copy in scattered:
+            across.append(copy)
+
+    send_w(1, (0,))
+
+    for copy in across:
+        copy.wait_recv()
+    for acc, part, near, got in pairs:
+        for z in range(zs):
+            start = pl.multiple_of((z * ys + my_y) * ranks, ranks)
+            value = acc[pl.ds(start, ranks), :]
+            for d in range(ys - 1):
+                value = value + near[d, z].astype(jnp.float32)
+            acc[pl.ds(start, ranks), :] = value
+            near[ys - 1, z] = value.astype(jnp.bfloat16)
+    along = []
+    for d in range(1, zs):
+        other = lax.rem(my_z + d, zs)
+        for k, (acc, part, near, got) in enumerate(pairs):
+            copy = remote(
+                near.at[ys - 1, other],
+                got.at[d - 1],
+                r_send.at[d - 1, k],
+                r_recv.at[d - 1, k],
+                other * ys + my_y,
+            )
+            copy.start()
+            along.append(copy)
+
+    send_w(1, (1,))
+
+    for copy in along:
         copy.wait_recv()
     kept = pl.ds(pl.multiple_of(me * ranks, ranks), ranks)
     for acc, got, low_ref, m_ref, v_ref, u_ref in (
@@ -219,39 +289,68 @@
         (acc_v, got_v, lowv_ref, mv_ref, vv_ref, uv_ref),
     ):
         low = acc[kept, :]
-        for d in range(n - 1):
+        for d in range(zs - 1):
             low = low + got[d].astype(jnp.float32)
         low_ref[...] = low
         u_ref[kept, :] = update_of(low, m_ref[...], v_ref[...]).astype(jnp.bfloat16)
 
+    def block(z, y):
+        return pl.ds(pl.multiple_of((z * ys + y) * ranks, ranks), ranks)
+
     gathered = []
-    for d in range(1, n):
+    for d in range(1, zs):
         for k, u_ref in enumerate((uq_ref, uv_ref)):
-            copy = pltpu.make_async_remote_copy(
-                src_ref=u_ref.at[kept],
-                dst_ref=u_ref.at[kept],
-                send_sem=u_send.at[d - 1, k],
-                recv_sem=u_recv.at[d - 1, k],
-                device_id={"fs": lax.rem(me + d, n)},
-                device_id_type=pl.DeviceIdType.MESH,
+            copy = remote(
+                u_ref.at[kept],
+                u_ref.at[kept],
+                u_send.at[d - 1, k],
+                u_recv.at[d - 1, k],
+                lax.rem(my_z + d, zs) * ys + my_y,
             )
             copy.start()
             gathered.append(copy)
 
-    send_w(2)
-
-    for d in range(1, n):
-        source = lax.rem(me - d + n, n)
-        chunk = pl.ds(pl.multiple_of(source * ranks, ranks), ranks)
+    def forward(z, s):
+        for d in range(1, ys):
+            for k, u_ref in enumerate((uq_ref, uv_ref)):
+                copy = remote(
+                    u_ref.at[block(z, my_y)],
+                    u_ref.at[block(z, my_y)],
+                    f_send.at[d - 1, s, k],
+                    f_recv.at[d - 1, s, k],
+                    my_z * ys + lax.rem(my_y + d, ys),
+                )
+                copy.start()
+                gathered.append(copy)
+
+    forward(my_z, 0)
+
+    send_w(2, (0,))
+
+    for d in range(1, zs):
+        source = lax.rem(my_z - d + zs, zs)
         for k, u_ref in enumerate((uq_ref, uv_ref)):
-            pltpu.make_async_remote_copy(
-                src_ref=u_ref.at[chunk],
-                dst_ref=u_ref.at[chunk],
-                send_sem=u_send.at[d - 1, k],
-                recv_sem=u_recv.at[d - 1, k],
-                device_id={"fs": source},
-                device_id_type=pl.DeviceIdType.MESH,
+            rows_ = u_ref.at[block(source, my_y)]
+            remote(
+                rows_, rows_, u_send.at[d - 1, k], u_recv.at[d - 1, k], source * ys + my_y
             ).wait_recv()
+        forward(source, d)
+
+    send_w(2, (1,))
+
+    for d in range(1, ys):
+        source = lax.rem(my_y - d + ys, ys)
+        for s in range(zs):
+            row = lax.rem(my_z - s + zs, zs)
+            for k, u_ref in enumerate((uq_ref, uv_ref)):
+                rows_ = u_ref.at[block(row, source)]
+                remote(
+                    rows_,
+                    rows_,
+                    f_send.at[d - 1, s, k],
+                    f_recv.at[d - 1, s, k],
+                    my_z * ys + source,
+                ).wait_recv()
 
     square = jnp.float32(0)
     for u_ref in (uq_ref, uv_ref):
@@ -279,7 +378,7 @@
     total_ref[...] = jnp.sum(sums[...], axis=0)
     for copy in own:
         copy.wait()
-    for copy in started + scattered + gathered + shared:
+    for copy in started + across + along + gathered + shared:
         copy.wait_send()
 
 
@@ -298,6 +397,8 @@
     anywhere = pl.BlockSpec(memory_space=pl.ANY)
     inside = pl.BlockSpec(memory_space=pltpu.VMEM)
     hops = n // 2
+    zs = 4 if n % 4 == 0 else n
+    ys = n // zs
     gq, gv, uq, uv, lowq, lowv, total = pl.pallas_call(
         functools.partial(kernel, n, t, tile),
         out_shape=(
@@ -309,28 +410,41 @@
             jax.ShapeDtypeStruct((ranks, width_v), full),
             jax.ShapeDtypeStruct((8, 128), full),
         ),
-        in_specs=[anywhere] * 3 + [inside] * 8,
+        in_specs=[anywhere] * 5 + [inside] * 2 + [anywhere] * 4,
         out_specs=(anywhere,) * 2 + (inside,) * 5,
         scratch_shapes=[
             pltpu.VMEM((rank, width_q), full),
             pltpu.VMEM((rank, width_v), full),
-            pltpu.VMEM((rank, width_q), half),
-            pltpu.VMEM((rank, width_v), half),
-            pltpu.VMEM((n - 1, ranks, width_q), half),
-            pltpu.VMEM((n - 1, ranks, width_v), half),
+            pltpu.VMEM((zs, ys, ranks, width_q), half),
+            pltpu.VMEM((zs, ys, ranks, width_v), half),
+            pltpu.VMEM((ys, zs, ranks, width_q), half),
+            pltpu.VMEM((ys, zs, ranks, width_v), half),
+            pltpu.VMEM((zs - 1, ranks, width_q), half),
+            pltpu.VMEM((zs - 1, ranks, width_v), half),
             pltpu.VMEM((t, 8, 128), full),
+            pltpu.VMEM(proj_query.shape, half),
+            pltpu.VMEM(proj_value.shape, half),
+            pltpu.VMEM(m_query.shape, full),
+            pltpu.VMEM(m_value.shape, full),
+            pltpu.VMEM(v_query.shape, full),
+            pltpu.VMEM(v_value.shape, full),
+            pltpu.SemaphoreType.DMA((6,)),
+            pltpu.SemaphoreType.DMA((max(ys - 1, 1), 2)),
+            pltpu.SemaphoreType.DMA((max(ys - 1, 1), 2)),
+            pltpu.SemaphoreType.DMA((max(ys - 1, 1), zs, 2)),
+            pltpu.SemaphoreType.DMA((max(ys - 1, 1), zs, 2)),
             pltpu.SemaphoreType.DMA((2, 2, hops, 2)),
             pltpu.SemaphoreType.DMA((2, 2, hops, 2)),
             pltpu.SemaphoreType.DMA((2,)),
-            pltpu.SemaphoreType.DMA((n - 1, 2)),
-            pltpu.SemaphoreType.DMA((n - 1, 2)),
-            pltpu.SemaphoreType.DMA((n - 1, 2)),
-            pltpu.SemaphoreType.DMA((n - 1, 2)),
+            pltpu.SemaphoreType.DMA((zs - 1, 2)),
+            pltpu.SemaphoreType.DMA((zs - 1, 2)),
+            pltpu.SemaphoreType.DMA((zs - 1, 2)),
+            pltpu.SemaphoreType.DMA((zs - 1, 2)),
             pltpu.SemaphoreType.DMA((t - 1,)),
             pltpu.SemaphoreType.DMA((t - 1,)),
         ],
         compiler_params=pltpu.CompilerParams(
-            collective_id=0, has_side_effects=True, vmem_limit_bytes=48 * 2**20
+            collective_id=0, has_side_effects=True, vmem_limit_bytes=60 * 2**20
         ),
     )(
         inputs, cot_query, cot_value, proj_query, proj_value,

time: 129 us -> 114 us (0.88)
  Pallas kernels: 105 us -> 92.5 us
  local copies, waits for them, and re-layouts: 6.45 us -> 1.26 us
  other arithmetic: 3.78 us -> 5.29 us
    pallas_call x1, Pallas kernels: 105 us -> 92.5 us  [on_device(): pl.pallas_call(functools.partial(kernel, n, t, tile), out_shape=(jax.Shap...]
    unnamed x18 -> x26, local copies, waits for them, and re-layouts: 5.94 us -> 0.07 us
where the time goes in v2:
time: 114 us; the launch traced here: 112 us
  Pallas kernels  92.5 us (81%)
  matrix products  11.7 us (10%)
  other arithmetic  5.29 us (5%)
  between operations  1.47 us (1%)
  local copies, waits for them, and re-layouts  1.26 us (1%)
    pallas_call x1, Pallas kernels, on_device(): pl.pallas_call(functools.partial(kernel, n, t, tile), out_shape=(jax.Shap...  92.5 us
    dot_general x4, matrix products, dot(): return jnp.dot(a, b, preferred_element_type=full)  11.7 us

profile of v2, /device:TPU:4, one launch (start us, length us, event | category | flops | bytes accessed | tf_op | source)
XLA Modules:
  0.0 112.2 jit_solution(18292699949797692325)
XLA Ops:
  0.6 1.8 %convert_element_type.20.wq_ref = bf16[256,512]{1,0:T(8,128)(2,1)} convert(f32[256,512]{1,0:T(8,128)} %param.16) | non-fusion elementwise | flops 131072 | bytes 786432 | tf_op jit(solution)/shard_map/convert_element_type | solution.py:451
  2.4 2.1 %convert_element_type.21.wv_ref = bf16[256,1024]{1,0:T(8,128)(2,1)} convert(f32[256,1024]{1,0:T(8,128)} %param.17) | non-fusion elementwise | flops 262144 | bytes 1572864 | tf_op jit(solution)/shard_map/convert_element_type | solution.py:451
  4.5 0.0 copy-start.3
  4.5 92.5 %shard_map.186 = (bf16[2048,512]{1,0:T(8,128)(2,1)}, bf16[2048,1024]{1,0:T(8,128)(2,1)}, bf16[256,512]{1,0:T(8,128)(2,1)}, bf16[256,1024]{1,0:T(8,128)(2,1)}, f3...) custom-call(bf16[3072,2048]{1,0:T(8,128)(2,1)} %x_hbm.1, bf16[3072,512]{1,0:T(8,128)(2,1)} %cq_hbm.1, ...), custom_call_target="tpu_custom_call" | custom-call | tf_op jit(solution)/shard_map/pallas_call | solution.py:402
  97.0 1.2 %slice.3 = f32[1,1]{1,0:T(1,128)} slice(f32[8,128]{1,0:T(8,128)} %get-tuple-element.17), slice={[0:1], [0:1]} | slice | bytes 8 | tf_op jit(solution)/shard_map/slice | solution.py:457
  98.9 0.0 copy-done.3
  98.9 0.0 copy-start.2
  98.9 0.0 copy-start.9
  99.0 0.0 copy-start.12
  99.0 6.5 %fusion.2 = bf16[2048,1024]{1,0:T(8,128)(2,1)} fusion(bf16[2048,1024]{1,0:T(8,128)(2,1)} %get-tuple-element.21, bf16[2048,256]{1,0:T(8,128)(2,1)S(1)} %copy-done.3, bf16[256,1024]{1,0:T(8,128)(2,1)} %get-tuple-element.19, f32[]{:T(128)} %bitcast), kind=kOutput, calls=%fused_computation.4 | convolution fusion | flops 1088421888 | bytes 9961476 | tf_op jit(solution)/shard_map/dot_general | solution.py:463
  105.4 0.0 copy-done.2
  105.4 0.0 copy-done.9
  105.4 0.0 copy-done.12
  105.4 0.0 copy-start.7
  105.5 0.0 copy-start.8
  105.5 0.0 copy-start.11
  105.5 0.0 copy-start.4
  105.5 0.0 copy-start.5
  105.5 0.0 copy-start.10
  105.5 0.0 copy-start.1
  105.5 0.0 copy-start
  105.5 0.0 copy-start.6
  105.5 2.4 %fusion.5 = bf16[2048,512]{1,0:T(8,128)(2,1)} fusion(bf16[2048,512]{1,0:T(8,128)(2,1)S(1)} %copy-done.12, bf16[2048,256]{1,0:T(8,128)(2,1)S(1)} %copy-done.2, bf16[256,512]{1,0:T(8,128)(2,1)S(1)} %copy-done.9, f32[]{:T(128)} %bitcast), kind=kOutput, calls=%fused_computation.9 | convolution fusion | flops 544210944 | bytes 5505028 | tf_op jit(solution)/shard_map/dot_general | solution.py:463
  107.9 0.0 copy-done.7
  107.9 0.0 copy-done.8
  107.9 0.0 copy-done.11
  107.9 0.7 fusion.11
  108.6 0.0 copy-done.4
  108.6 0.0 copy-done.5
  108.6 0.0 copy-done.10
  108.6 0.7 fusion.8
  109.3 0.0 copy-done.1
  109.3 1.2 %multiply_subtract_fusion.1 = (f32[256,512]{1,0:T(8,128)}, f32[256,512]{1,0:T(8,128)}) fusion(f32[256,512]{1,0:T(8,128)S(1)} %copy-done.1, bf16[256,512]{1,0:T(8,128)(2,1)S(1)} %copy-done.9, bf16[2048,256]{1,0:T(8,128)(2,1)S(1)} %copy-done.2, s32[]{:T(128)S(6)} %select_n.4, f32[]{:T(128)} %bitcast), kind=kOutput, calls=%fused_computation.15 | convolution fusion | flops 67764224 | bytes 1966088 | tf_op jit(solution)/shard_map/dot_general | solution.py:463
  110.6 0.0 copy-done
  110.6 0.0 copy-done.6
  110.6 1.7 %multiply_subtract_fusion = (f32[256,1024]{1,0:T(8,128)}, f32[256,1024]{1,0:T(8,128)}) fusion(f32[256,1024]{1,0:T(8,128)S(1)} %copy-done, bf16[256,1024]{1,0:T(8,128)(2,1)S(1)} %copy-done.6, bf16[2048,256]{1,0:T(8,128)(2,1)S(1)} %copy-done.3, s32[]{:T(128)S(6)} %select_n.4, f32[]{:T(128)} %bitcast), kind=kOutput, calls=%fused_computation.14 | convolution fusion | flops 135528448 | bytes 3801096 | tf_op jit(solution)/shard_map/dot_general | solution.py:463
Async XLA Ops:
  4.5 94.4 %copy-start.3 = (bf16[2048,256]{1,0:T(8,128)(2,1)S(1)}, bf16[2048,256]{1,0:T(8,128)(2,1)}, u32[]{:S(2)}) copy-start(bf16[2048,256]{1,0:T(8,128)(2,1)} %pv_hbm.1) | copy-start | bytes 3145732
  98.9 6.5 %copy-start.2 = (bf16[2048,256]{1,0:T(8,128)(2,1)S(1)}, bf16[2048,256]{1,0:T(8,128)(2,1)}, u32[]{:S(2)}) copy-start(bf16[2048,256]{1,0:T(8,128)(2,1)} %pq_hbm.1) | copy-start | bytes 3145732
  98.9 6.5 %copy-start.9 = (bf16[256,512]{1,0:T(8,128)(2,1)S(1)}, bf16[256,512]{1,0:T(8,128)(2,1)}, u32[]{:S(2)}) copy-start(bf16[256,512]{1,0:T(8,128)(2,1)} %get-tuple-element.18) | copy-start | bytes 786436
  99.0 6.5 %copy-start.12 = (bf16[2048,512]{1,0:T(8,128)(2,1)S(1)}, bf16[2048,512]{1,0:T(8,128)(2,1)}, u32[]{:S(2)}) copy-start(bf16[2048,512]{1,0:T(8,128)(2,1)} %get-tuple-element.20) | copy-start | bytes 6291460
  105.4 2.5 %copy-start.7 = (f32[32,512]{1,0:T(8,128)S(1)}, f32[32,512]{1,0:T(8,128)}, u32[]{:S(2)}) copy-start(f32[32,512]{1,0:T(8,128)} %mq_hbm.1) | copy-start | bytes 196612
  105.5 2.4 %copy-start.8 = (f32[32,512]{1,0:T(8,128)S(1)}, f32[32,512]{1,0:T(8,128)}, u32[]{:S(2)}) copy-start(f32[32,512]{1,0:T(8,128)} %vq_hbm.1) | copy-start | bytes 196612
  105.5 2.4 %copy-start.11 = (f32[32,512]{1,0:T(8,128)S(1)}, f32[32,512]{1,0:T(8,128)}, u32[]{:S(2)}) copy-start(f32[32,512]{1,0:T(8,128)} %get-tuple-element.22) | copy-start | bytes 196612
  105.5 3.1 %copy-start.4 = (f32[32,1024]{1,0:T(8,128)S(1)}, f32[32,1024]{1,0:T(8,128)}, u32[]{:S(2)}) copy-start(f32[32,1024]{1,0:T(8,128)} %mv_hbm.1) | copy-start | bytes 393220
  105.5 3.1 %copy-start.5 = (f32[32,1024]{1,0:T(8,128)S(1)}, f32[32,1024]{1,0:T(8,128)}, u32[]{:S(2)}) copy-start(f32[32,1024]{1,0:T(8,128)} %vv_hbm.1) | copy-start | bytes 393220
  105.5 3.1 %copy-start.10 = (f32[32,1024]{1,0:T(8,128)S(1)}, f32[32,1024]{1,0:T(8,128)}, u32[]{:S(2)}) copy-start(f32[32,1024]{1,0:T(8,128)} %get-tuple-element.23) | copy-start | bytes 393220
  105.5 3.8 %copy-start.1 = (f32[256,512]{1,0:T(8,128)S(1)}, f32[256,512]{1,0:T(8,128)}, u32[]{:S(2)}) copy-start(f32[256,512]{1,0:T(8,128)} %param.16) | copy-start | bytes 1572868
  105.5 5.0 %copy-start = (f32[256,1024]{1,0:T(8,128)S(1)}, f32[256,1024]{1,0:T(8,128)}, u32[]{:S(2)}) copy-start(f32[256,1024]{1,0:T(8,128)} %param.17) | copy-start | bytes 3145732
  105.5 5.0 %copy-start.6 = (bf16[256,1024]{1,0:T(8,128)(2,1)S(1)}, bf16[256,1024]{1,0:T(8,128)(2,1)}, u32[]{:S(2)}) copy-start(bf16[256,1024]{1,0:T(8,128)(2,1)} %get-tuple-element.19) | copy-start | bytes 1572868
